TPU v7x, 512 devices: a whole 4x8x8 slice. The times are simulated.
512 devices in a mesh: rep: 2 (over z_hi), fs: 32 (over z_lo, y), tp: 8 (over x, core).
Axes of the slice: x: 4, y: 8, z: 8 (z_hi: 2, z_lo: 4; z = z_hi * 4 + z_lo), core: 2. Of those that a mesh axis runs over, the one named last changes fastest.
Arguments:
- x_early: bfloat16 [7168, 2048], P(('rep', 'fs')), may hold values from -6 to 6
- x_late: bfloat16 [7168, 2048], P(('rep', 'fs')), may hold values from -6 to 6
- grad_out: bfloat16 [7168, 2048], P(('rep', 'fs')), may hold values from -16 to 16
- w_gate: bfloat16 [2048, 3072], P('fs', 'tp'), may hold values from -0.125 to 0.125
- w_up: bfloat16 [2048, 3072], P('fs', 'tp'), may hold values from -0.125 to 0.125
- w_down: bfloat16 [3072, 2048], P('tp', 'fs'), may hold values from -0.109375 to 0.109375
- gate_sum: float32 [2048, 3072], P('fs', 'tp'), may hold values from -160 to 160
- up_sum: float32 [2048, 3072], P('fs', 'tp'), may hold values from -160 to 160
- down_sum: float32 [3072, 2048], P('tp', 'fs'), may hold values from -160 to 160
Outputs:
- out_late: bfloat16 [7168, 2048], P(('rep', 'fs'))
- grad_in: bfloat16 [7168, 2048], P(('rep', 'fs'))
- new_gate_sum: float32 [2048, 3072], P('fs', 'tp')
- new_up_sum: float32 [2048, 3072], P('fs', 'tp')
- new_down_sum: float32 [3072, 2048], P('tp', 'fs')
All inputs are finite; a program needn't handle non-finite values.
Results may differ from a plain program's by a relative error of at most 0.018.
Values may be sent and summed in bfloat16 or wider, within the bound.
No kernel may reach another device: no remote copies, remote signals or barrier semaphores. Data moves between devices by JAX's collectives and lax.ppermute only.
A program may use at most 64 MiB of HBM per device.

v0:
```python
import jax
import jax.numpy as jnp
from jax import lax
from jax.sharding import PartitionSpec as P

epsilon = 1e-06


def rows_first(arrays, axis, dims):
    turned = [jnp.moveaxis(a, dim, 0) for a, dim in zip(arrays, dims)]
    both = jnp.concatenate([t.reshape(len(t), -1) for t in turned], axis=1)
    whole, at, gathered = (lax.all_gather(both, axis, axis=0, tiled=True), 0, [])
    for t, dim in zip(turned, dims):
        share = whole[:, at : at + t[0].size].reshape(-1, *t.shape[1:])
        gathered.append(jnp.moveaxis(share, 0, dim))
        at += t[0].size
    return tuple(gathered)


def from_everyone(value, axis):
    copies = jnp.broadcast_to(value, (lax.axis_size(axis), *value.shape))
    return lax.all_to_all(copies, axis, split_axis=0, concat_axis=0, tiled=True)


def taken_together(value, axis):
    return from_everyone(value, axis).astype(jnp.float32).sum(axis=0)


def filled_up(lines, length):
    spare = -len(lines) % length
    return jnp.pad(lines, [(0, spare)] + [(0, 0)] * (lines.ndim - 1))


def total_of(value, axis):
    lines = value.reshape(-1, *value.shape[1:][-1:])
    own = lax.psum_scatter(
        filled_up(lines, lax.axis_size(axis)), axis, scatter_dimension=0, tiled=True
    )
    whole = lax.all_gather(own, axis).reshape(-1, *lines.shape[1:])
    return lax.slice_in_dim(whole, 0, len(lines)).reshape(value.shape)


def sent_together(arrays, axis, dim, along):
    both = jnp.concatenate(arrays, axis=along)
    whole, at, gathered = (lax.all_gather(both, axis, axis=dim, tiled=True), 0, [])
    for a in arrays:
        gathered.append(lax.slice_in_dim(whole, at, at + a.shape[along], axis=along))
        at += a.shape[along]
    return tuple(gathered)


def contract_rows(left, right):
    return lax.dot_general(
        left, right, (((0,), (0,)), ((), ())), preferred_element_type=jnp.float32
    )


def contract_cols(left, right):
    return lax.dot_general(
        left, right, (((1,), (1,)), ((), ())), preferred_element_type=jnp.float32
    )


def shards(x_early, x_late, grad_out, w_gate, w_up, w_down, gate_sum, up_sum, down_sum):
    gate_full, up_full, down_full = rows_first((w_gate, w_up, w_down), "fs", (0, 0, 1))
    batch_rows = x_early.shape[0]
    stacked = jnp.concatenate([x_early, x_late], axis=0).astype(jnp.float32)
    row_scale = lax.rsqrt(jnp.mean(stacked * stacked, axis=-1, keepdims=True) + epsilon)
    normed = (stacked * row_scale).astype(jnp.bfloat16)
    gate_pre = jnp.dot(normed, gate_full, preferred_element_type=jnp.float32)
    up_pre = jnp.dot(normed, up_full, preferred_element_type=jnp.float32)
    gate_sig = jax.nn.sigmoid(gate_pre)
    hidden = (gate_pre * gate_sig * up_pre).astype(jnp.bfloat16)
    late_part = jnp.dot(hidden[batch_rows:], down_full, preferred_element_type=jnp.float32).astype(
        jnp.bfloat16
    )
    branch = taken_together(late_part, "tp").astype(jnp.float32)
    out_late = (stacked[batch_rows:] + 0.5 * branch).astype(jnp.bfloat16)
    early_gate = gate_pre[:batch_rows]
    early_upper = up_pre[:batch_rows]
    early_sig = gate_sig[:batch_rows]
    early_hidden = hidden[:batch_rows]
    early_normed = normed[:batch_rows]
    early_scale = row_scale[:batch_rows]
    grad_hidden = 0.5 * contract_cols(grad_out, down_full)
    grad_gate_in = (
        grad_hidden * early_upper * early_sig * (1.0 + early_gate * (1.0 - early_sig))
    ).astype(jnp.bfloat16)
    grad_up_in = (grad_hidden * early_gate * early_sig).astype(jnp.bfloat16)
    normed_part = contract_cols(grad_gate_in, gate_full) + contract_cols(grad_up_in, up_full)
    grad_normed = total_of(normed_part.astype(jnp.bfloat16), "tp").astype(jnp.float32)
    unit_rows = stacked[:batch_rows] * early_scale
    inner = jnp.mean(grad_normed * unit_rows, axis=-1, keepdims=True)
    grad_in = (
        grad_out.astype(jnp.float32) + early_scale * (grad_normed - unit_rows * inner)
    ).astype(jnp.bfloat16)
    normed_cols, out_cols = (
        lax.all_to_all(early_normed, "fs", split_axis=1, concat_axis=0, tiled=True),
        lax.all_to_all(grad_out, "fs", split_axis=1, concat_axis=0, tiled=True),
    )
    pieces = sent_together((grad_gate_in, grad_up_in, early_hidden), "fs", 0, 1)
    gate_delta = contract_rows(normed_cols, pieces[0])
    up_delta = contract_rows(normed_cols, pieces[1])
    down_half = contract_rows(pieces[2], out_cols)
    down_delta = 0.5 * down_half
    gate_delta, up_delta, down_delta = (
        taken_together(gate_delta.astype(jnp.bfloat16), "rep").astype(jnp.float32),
        taken_together(up_delta.astype(jnp.bfloat16), "rep").astype(jnp.float32),
        taken_together(down_delta.astype(jnp.bfloat16), "rep").astype(jnp.float32),
    )
    return (out_late, grad_in, gate_sum + gate_delta, up_sum + up_delta, down_sum + down_delta)


def solution(mesh):
    placed = (
        P(("rep", "fs"), None),
        P(("rep", "fs"), None),
        P(("rep", "fs"), None),
        P("fs", "tp"),
        P("fs", "tp"),
        P("tp", "fs"),
        P("fs", "tp"),
        P("fs", "tp"),
        P("tp", "fs"),
    )
    return jax.shard_map(
        shards,
        mesh=mesh,
        in_specs=placed,
        out_specs=(
            P(("rep", "fs"), None),
            P(("rep", "fs"), None),
            P("fs", "tp"),
            P("fs", "tp"),
            P("tp", "fs"),
        ),
        check_vma=False,
    )
```

profile of v0, /device:TPU:2, one launch (start us, length us, event | category | flops | bytes accessed | tf_op | source)
XLA Modules:
  0.0 403.2 jit_solution(4803687750171344934)
XLA Ops:
  7.2 0.0 all-gather.5.cloned.1.call-start
  7.2 1.5 pad_maximum_fusion.1
  8.7 0.0 all-gather.5.cloned.1.call-update
  8.8 0.0 all-gather.7.cloned.1.call-start
  8.8 1.4 multiply_reduce_fusion
  10.2 1.4 multiply_convert_fusion
  11.6 163.6 %all-gather.5.cloned.1.call-done = bf16[2048,1152]{1,0:T(8,128)(2,1)} async-done(((bf16[64,1152]{1,0:T(8,128)(2,1)}), bf16[2048,1152]{1,0:T(8,128)(2,1)}) %all-gather.5.cloned.1.call-update) | async-done | bytes 4718608 | tf_op jit(solution)/shard_map/all_gather | solution.py:12
  175.2 2.0 fusion.12
  177.2 0.0 copy-start.3
  177.2 2.1 add_divide_fusion
  179.4 0.0 copy-done.3
  179.4 1.9 multiply_convert_fusion.2
  181.3 0.7 pad_maximum_fusion
  182.0 0.0 all-gather.7.cloned.1.call-update
  182.1 1.0 copy.24
  183.1 9.5 %all-to-all-start.1 = ((bf16[112,32,64]{0,2,1:T(8,128)(2,1)}), bf16[112,32,64]{0,2,1:T(8,128)(2,1)S(1)}, u32[]{:S(2)}, u32[]{:S(2)}) async-start(bf16[112,32,64]{0,2,1:T(8,128)(2,1)} %bitcast.3), calls=%async_computation.1 | async-start | bytes 1048576 | tf_op jit(solution)/shard_map/all_to_all | solution.py:98
  192.6 1.0 copy.26
  193.6 16.0 %all-to-all-done.1 = bf16[112,32,64]{0,2,1:T(8,128)(2,1)S(1)} async-done(((bf16[112,32,64]{0,2,1:T(8,128)(2,1)}), bf16[112,32,64]{0,2,1:T(8,128)(2,1)S(1)}, u32[]{:S(2)}, u32[]{:S(2)}) %all-to-all-start.1) | async-done | bytes 458784 | tf_op jit(solution)/shard_map/all_to_all | solution.py:98
  209.6 6.4 %all-to-all-start.4 = ((bf16[112,32,64]{0,2,1:T(8,128)(2,1)}), bf16[112,32,64]{0,2,1:T(8,128)(2,1)S(1)}, u32[]{:S(2)}, u32[]{:S(2)}) async-start(bf16[112,32,64]{0,2,1:T(8,128)(2,1)} %bitcast.5), calls=%async_computation.4 | async-start | bytes 1048576 | tf_op jit(solution)/shard_map/all_to_all | solution.py:99
  216.1 2.0 convolution_convert_fusion
  218.1 15.3 %all-to-all-done.4 = bf16[112,32,64]{0,2,1:T(8,128)(2,1)S(1)} async-done(((bf16[112,32,64]{0,2,1:T(8,128)(2,1)}), bf16[112,32,64]{0,2,1:T(8,128)(2,1)S(1)}, u32[]{:S(2)}, u32[]{:S(2)}) %all-to-all-start.4) | async-done | bytes 458784 | tf_op jit(solution)/shard_map/all_to_all | solution.py:99
  233.4 2.3 broadcast_in_dim.14
  235.6 0.0 copy-done.2
  235.6 5.0 %all-to-all-start = ((bf16[8,112,2048]{2,1,0:T(8,128)(2,1)}), bf16[8,112,2048]{2,1,0:T(8,128)(2,1)}, u32[]{:S(2)}, u32[]{:S(2)}) async-start(bf16[8,112,2048]{2,1,0:T(8,128)(2,1)} %broadcast_in_dim.14), calls=%async_computation | async-start | bytes 7340032 | tf_op jit(solution)/shard_map/all_to_all | solution.py:22
  240.6 2.1 fusion.14
  242.7 2.0 fusion.7
  244.7 47.1 %fusion = bf16[16,2048]{1,0:T(8,128)(2,1)S(1)} fusion(bf16[112,2048]{1,0:T(8,128)(2,1)S(1)} %fusion.7), kind=kCustom, calls=%all-reduce-scatter | all-reduce-scatter fusion | flops 262145 | bytes 526336
  291.9 1.9 collective-permute-start
  293.8 0.0 copy-done
  293.8 0.0 copy-done.1
  293.8 0.2 maximum_convert_fusion
  294.0 1.3 dynamic-slice.4
  296.0 0.3 copy.25
  296.3 1.8 all_to_all.44
  298.1 1.4 copy.27
  299.5 1.8 all_to_all.50
  301.2 0.0 collective-permute-done
  301.2 0.2 concatenate.12
  301.5 13.2 %all-gather.1 = bf16[8,14,2048]{2,1,0:T(8,128)(2,1)S(1)} all-gather(bf16[1,14,2048]{2,1,0:T(8,128)(2,1)S(1)} %dynamic-slice_bitcast_fusion), channel_id=2, replica_groups=mesh['rep'=2,'fs'=32,'tp'=8] {'tp'}, dimensions={0}, use_global_device_ids=true | all-gather | bytes 516096 | tf_op jit(solution)/shard_map/all_gather | solution.py:39
  314.7 0.1 reshape.52
  314.8 0.2 multiply_reduce_fusion.1
  315.0 0.0 all-to-all-done
  315.1 2.9 convert_reduce_fusion
  317.9 1.2 add_convert_fusion
  319.1 37.0 %all-gather.7.cloned.1.call-done = bf16[3584,1152]{1,0:T(8,128)(2,1)} async-done(((bf16[112,1152]{1,0:T(8,128)(2,1)}), bf16[3584,1152]{1,0:T(8,128)(2,1)}) %all-gather.7.cloned.1.call-update) | async-done | bytes 8257552 | tf_op jit(solution)/shard_map/all_gather | solution.py:45
  356.2 2.5 fusion.30
  358.7 0.7 broadcast_in_dim.15
  359.3 3.4 all-to-all-start.2
  362.7 2.3 fusion.33
  365.0 0.0 copy-start.7
  365.0 0.0 copy-start.8
  365.0 0.0 copy-start.9
  365.1 2.4 fusion.27
  367.4 3.5 all-to-all-done.2
  370.9 0.6 broadcast_in_dim.16
  371.5 3.8 all-to-all-start.3
  375.3 0.0 copy-done.7
  375.3 0.7 add.49
  376.0 7.5 %all-to-all-done.3 = bf16[2,64,384]{2,1,0:T(8,128)(2,1)S(1)} async-done(((bf16[2,64,384]{2,1,0:T(8,128)(2,1)}), bf16[2,64,384]{2,1,0:T(8,128)(2,1)S(1)}, u32[]{:S(2)}, u32[]{:S(2)}) %all-to-all-start.3) | async-done | bytes 98336 | tf_op jit(solution)/shard_map/all_to_all | solution.py:22
  383.5 0.6 broadcast_in_dim.17
  384.1 3.3 all-to-all-start.5
  387.5 0.7 add.50
  388.2 7.5 %all-to-all-done.5 = bf16[2,384,64]{1,2,0:T(8,128)(2,1)S(1)} async-done(((bf16[2,384,64]{1,2,0:T(8,128)(2,1)}), bf16[2,384,64]{1,2,0:T(8,128)(2,1)S(1)}, u32[]{:S(2)}, u32[]{:S(2)}) %all-to-all-start.5) | async-done | bytes 98336 | tf_op jit(solution)/shard_map/all_to_all | solution.py:22
  395.7 0.7 add.51
  (21 shorter events, 0.2 us)
Async XLA Ops:
  7.2 168.0 %all-gather.5.cloned.1.call-start = ((), (), s32[]{:S(2)}) async-start(), calls=%async_computation.6 | async-start | bytes 4866048 | tf_op jit(solution)/shard_map/all_gather | solution.py:12
  8.8 347.4 %all-gather.7.cloned.1.call-start = ((), (), s32[]{:S(2)}) async-start(), calls=%async_computation.7 | async-start | bytes 8515584 | tf_op jit(solution)/shard_map/all_gather | solution.py:45
  177.2 2.2 copy-start.3
  183.1 26.5 %all-to-all-start.1 = ((bf16[112,32,64]{0,2,1:T(8,128)(2,1)}), bf16[112,32,64]{0,2,1:T(8,128)(2,1)S(1)}, u32[]{:S(2)}, u32[]{:S(2)}) async-start(bf16[112,32,64]{0,2,1:T(8,128)(2,1)} %bitcast.3), calls=%async_computation.1 | async-start | bytes 1048576 | tf_op jit(solution)/shard_map/all_to_all | solution.py:98
  209.6 23.8 %all-to-all-start.4 = ((bf16[112,32,64]{0,2,1:T(8,128)(2,1)}), bf16[112,32,64]{0,2,1:T(8,128)(2,1)S(1)}, u32[]{:S(2)}, u32[]{:S(2)}) async-start(bf16[112,32,64]{0,2,1:T(8,128)(2,1)} %bitcast.5), calls=%async_computation.4 | async-start | bytes 1048576 | tf_op jit(solution)/shard_map/all_to_all | solution.py:99
  233.4 2.3 copy-start.2
  235.6 79.4 %all-to-all-start = ((bf16[8,112,2048]{2,1,0:T(8,128)(2,1)}), bf16[8,112,2048]{2,1,0:T(8,128)(2,1)}, u32[]{:S(2)}, u32[]{:S(2)}) async-start(bf16[8,112,2048]{2,1,0:T(8,128)(2,1)} %broadcast_in_dim.14), calls=%async_computation | async-start | bytes 7340032 | tf_op jit(solution)/shard_map/all_to_all | solution.py:22
  240.6 53.2 %copy-start = (bf16[112,2048]{1,0:T(8,128)(2,1)S(1)}, bf16[112,2048]{1,0:T(8,128)(2,1)}, u32[]{:S(2)}) copy-start(bf16[112,2048]{1,0:T(8,128)(2,1)} %param.10) | copy-start | bytes 1376260
  240.6 53.2 %copy-start.1 = (bf16[112,2048]{1,0:T(8,128)(2,1)S(1)}, bf16[112,2048]{1,0:T(8,128)(2,1)}, u32[]{:S(2)}) copy-start(bf16[112,2048]{1,0:T(8,128)(2,1)} %param.9) | copy-start | bytes 1376260
  291.9 9.4 %collective-permute-start = (bf16[14,2048]{1,0:T(8,128)(2,1)S(1)}, bf16[14,2048]{1,0:T(8,128)(2,1)S(1)}, u32[]{:S(2)}, u32[]{:S(2)}) collective-permute-start(bf16[14,2048]{1,0:T(8,128)(2,1)S(1)} %slice.75), channel_id=1, source_target_pairs={{0,1},{1,2},{2,3},{3,4},{4,5},{5,6},{6,7},{8,9},{9,10},{10,11},{11... | collective-permute-start | bytes 172040
  315.0 2.9 copy-start.4
  319.1 43.5 %copy-start.5 = (bf16[3584,64]{0,1:T(8,128)(2,1)S(1)}, bf16[3584,64]{0,1:T(8,128)(2,1)}, u32[]{:S(2)}) copy-start(bf16[3584,64]{0,1:T(8,128)(2,1)} %all_to_all.44) | copy-start | bytes 1376260
  358.7 6.4 %copy-start.6 = (bf16[3584,64]{0,1:T(8,128)(2,1)S(1)}, bf16[3584,64]{0,1:T(8,128)(2,1)}, u32[]{:S(2)}) copy-start(bf16[3584,64]{0,1:T(8,128)(2,1)} %all_to_all.50) | copy-start | bytes 1376260
  359.3 11.6 %all-to-all-start.2 = ((bf16[2,64,384]{2,1,0:T(8,128)(2,1)}), bf16[2,64,384]{2,1,0:T(8,128)(2,1)S(1)}, u32[]{:S(2)}, u32[]{:S(2)}) async-start(bf16[2,64,384]{2,1,0:T(8,128)(2,1)} %broadcast_in_dim.15), calls=%async_computation.2 | async-start | bytes 196608 | tf_op jit(solution)/shard_map/all_to_all | solution.py:22
  365.0 10.3 %copy-start.7 = (f32[64,384]{1,0:T(8,128)S(1)}, f32[64,384]{1,0:T(8,128)}, u32[]{:S(2)}) copy-start(f32[64,384]{1,0:T(8,128)} %param.15) | copy-start | bytes 294916
  365.0 22.5 %copy-start.8 = (f32[64,384]{1,0:T(8,128)S(1)}, f32[64,384]{1,0:T(8,128)}, u32[]{:S(2)}) copy-start(f32[64,384]{1,0:T(8,128)} %param.16) | copy-start | bytes 294916
  365.0 30.7 %copy-start.9 = (f32[384,64]{0,1:T(8,128)S(1)}, f32[384,64]{0,1:T(8,128)}, u32[]{:S(2)}) copy-start(f32[384,64]{0,1:T(8,128)} %param.17) | copy-start | bytes 294916
  371.5 12.0 %all-to-all-start.3 = ((bf16[2,64,384]{2,1,0:T(8,128)(2,1)}), bf16[2,64,384]{2,1,0:T(8,128)(2,1)S(1)}, u32[]{:S(2)}, u32[]{:S(2)}) async-start(bf16[2,64,384]{2,1,0:T(8,128)(2,1)} %broadcast_in_dim.16), calls=%async_computation.3 | async-start | bytes 196608 | tf_op jit(solution)/shard_map/all_to_all | solution.py:22
  384.1 11.5 %all-to-all-start.5 = ((bf16[2,384,64]{1,2,0:T(8,128)(2,1)}), bf16[2,384,64]{1,2,0:T(8,128)(2,1)S(1)}, u32[]{:S(2)}, u32[]{:S(2)}) async-start(bf16[2,384,64]{1,2,0:T(8,128)(2,1)} %broadcast_in_dim.17), calls=%async_computation.5 | async-start | bytes 196608 | tf_op jit(solution)/shard_map/all_to_all | solution.py:22
Sparse Core Ops, SparseCore 0:
  10.6 164.5 all-gather.4
  182.1 173.9 all-gather.6
where the time goes:
time: 404 us; the launch traced here: 403 us
  waiting for transfers between devices  250 us (62%)
  blocking collectives  60.3 us (15%)
  starting transfers between devices  33.4 us (8%)
  matrix products  19.3 us (5%)
  between operations  15 us (4%)
  local copies, waits for them, and re-layouts  13.2 us (3%)
  other arithmetic  11.6 us (3%)
    all_gather x1, waiting for transfers between devices, rows_first(): lax.all_gather(both, axis, axis=0, tiled=True)  164 us
    unnamed x1, blocking collectives  47.1 us
    all_gather x1, waiting for transfers between devices, sent_together(): lax.all_gather(both, axis, axis=dim, tiled=True)  37 us
    all_to_all x4, waiting for transfers between devices, from_everyone(): return lax.all_to_all(copies, axis, split_axis=0, concat_axis=0, tiled=True)  18.5 us
    all_to_all x1, waiting for transfers between devices, shards(): lax.all_to_all(early_normed, 'fs', split_axis=1, concat_axis=0, tiled=True)  16 us
    all_to_all x4, starting transfers between devices, from_everyone(): return lax.all_to_all(copies, axis, split_axis=0, concat_axis=0, tiled=True)  15.4 us
    all_to_all x1, waiting for transfers between devices, shards(): lax.all_to_all(grad_out, 'fs', split_axis=1, concat_axis=0, tiled=True)  15.3 us
    all_gather x1, blocking collectives, total_of(): whole = lax.all_gather(own, axis).reshape(-1, *lines.shape[1:])  13.2 us
  transfers between devices with their start and end apart: 9, of which 7 were waited for; matrix products, arithmetic and copies ran while one was open for 18% of the time, Pallas kernels for 0%

commit v1 on v0

--- a/solution.py
+++ b/solution.py
@@ -9,7 +9,13 @@
 def rows_first(arrays, axis, dims):
     turned = [jnp.moveaxis(a, dim, 0) for a, dim in zip(arrays, dims)]
     both = jnp.concatenate([t.reshape(len(t), -1) for t in turned], axis=1)
-    whole, at, gathered = (lax.all_gather(both, axis, axis=0, tiled=True), 0, [])
+    whole, at, gathered = (
+        jnp.concatenate(
+            lax.all_to_all(jnp.stack([both] * lax.axis_size(axis)), axis, 0, 0), axis=0
+        ),
+        0,
+        [],
+    )
     for t, dim in zip(turned, dims):
         share = whole[:, at : at + t[0].size].reshape(-1, *t.shape[1:])
         gathered.append(jnp.moveaxis(share, 0, dim))

time: 404 us -> 388 us (0.960)
  the two profiles are of different devices: /device:TPU:2 before, /device:TPU:6 now
where the time goes in v1:
time: 388 us; the launch traced here: 387 us
  waiting for transfers between devices  216 us (56%)
  blocking collectives  60.3 us (16%)
  starting transfers between devices  51.8 us (13%)
  matrix products  19.3 us (5%)
  local copies, waits for them, and re-layouts  16 us (4%)
  between operations  15 us (4%)
  other arithmetic  8.59 us (2%)
    all_to_all x1, waiting for transfers between devices, rows_first(): lax.all_to_all(jnp.stack([both] * lax.axis_size(axis)), axis, 0, 0)  120 us
    unnamed x1, blocking collectives  47.2 us
    all_gather x1, waiting for transfers between devices, sent_together(): lax.all_gather(both, axis, axis=dim, tiled=True)  38.8 us
    all_to_all x1, waiting for transfers between devices, shards(): lax.all_to_all(grad_out, 'fs', split_axis=1, concat_axis=0, tiled=True)  19.2 us
    all_to_all x1, waiting for transfers between devices, shards(): lax.all_to_all(early_normed, 'fs', split_axis=1, concat_axis=0, tiled=True)  19.2 us
    all_to_all x4, starting transfers between devices, from_everyone(): return lax.all_to_all(copies, axis, split_axis=0, concat_axis=0, tiled=True)  19.1 us
    all_to_all x4, waiting for transfers between devices, from_everyone(): return lax.all_to_all(copies, axis, split_axis=0, concat_axis=0, tiled=True)  18.5 us
    all_to_all x1, starting transfers between devices, rows_first(): lax.all_to_all(jnp.stack([both] * lax.axis_size(axis)), axis, 0, 0)  13.2 us
  transfers between devices with their start and end apart: 9, of which 7 were waited for; matrix products, arithmetic and copies ran while one was open for 19% of the time, Pallas kernels for 0%

profile of v1, /device:TPU:6, one launch (start us, length us, event | category | flops | bytes accessed | tf_op | source)
XLA Modules:
  0.0 387.0 jit_solution(5191975285264908568)
XLA Ops:
  7.2 0.9 pad_maximum_fusion.1
  8.0 2.8 stack.2
  10.8 13.2 %all-to-all-start = ((bf16[32,64,1152]{2,1,0:T(8,128)(2,1)}), bf16[32,64,1152]{2,1,0:T(8,128)(2,1)}, u32[]{:S(2)}, u32[]{:S(2)}) async-start(bf16[32,64,1152]{2,1,0:T(8,128)(2,1)} %stack.2), calls=%async_computation | async-start | bytes 9437184 | tf_op jit(solution)/shard_map/all_to_all | solution.py:14
  24.0 0.0 all-gather.4.cloned.1.call-start
  24.0 0.0 copy-done
  24.1 0.0 copy-done.1
  24.1 0.3 multiply_reduce_fusion
  24.3 0.2 multiply_convert_fusion
  24.6 120.3 %all-to-all-done = bf16[32,64,1152]{2,1,0:T(8,128)(2,1)} async-done(((bf16[32,64,1152]{2,1,0:T(8,128)(2,1)}), bf16[32,64,1152]{2,1,0:T(8,128)(2,1)}, u32[]{:S(2)}, u32[]{:S(2)}) %all-to-all-start) | async-done | bytes 4718624 | tf_op jit(solution)/shard_map/all_to_all | solution.py:14
  144.9 2.0 fusion.12
  146.9 0.0 copy-start.3
  146.9 2.1 add_divide_fusion
  149.1 0.0 copy-done.3
  149.1 1.9 multiply_convert_fusion.2
  151.0 0.7 pad_maximum_fusion
  151.7 0.0 all-gather.4.cloned.1.call-update
  151.7 1.0 copy.24
  152.8 12.5 %all-to-all-start.2 = ((bf16[112,32,64]{0,2,1:T(8,128)(2,1)}), bf16[112,32,64]{0,2,1:T(8,128)(2,1)S(1)}, u32[]{:S(2)}, u32[]{:S(2)}) async-start(bf16[112,32,64]{0,2,1:T(8,128)(2,1)} %bitcast.4), calls=%async_computation.2 | async-start | bytes 1048576 | tf_op jit(solution)/shard_map/all_to_all | solution.py:104
  165.3 1.0 copy.26
  166.3 19.2 %all-to-all-done.2 = bf16[112,32,64]{0,2,1:T(8,128)(2,1)S(1)} async-done(((bf16[112,32,64]{0,2,1:T(8,128)(2,1)}), bf16[112,32,64]{0,2,1:T(8,128)(2,1)S(1)}, u32[]{:S(2)}, u32[]{:S(2)}) %all-to-all-start.2) | async-done | bytes 458784 | tf_op jit(solution)/shard_map/all_to_all | solution.py:104
  185.5 5.1 %all-to-all-start.5 = ((bf16[112,32,64]{0,2,1:T(8,128)(2,1)}), bf16[112,32,64]{0,2,1:T(8,128)(2,1)S(1)}, u32[]{:S(2)}, u32[]{:S(2)}) async-start(bf16[112,32,64]{0,2,1:T(8,128)(2,1)} %bitcast.6), calls=%async_computation.5 | async-start | bytes 1048576 | tf_op jit(solution)/shard_map/all_to_all | solution.py:105
  190.6 2.0 convolution_convert_fusion
  192.6 19.2 %all-to-all-done.5 = bf16[112,32,64]{0,2,1:T(8,128)(2,1)S(1)} async-done(((bf16[112,32,64]{0,2,1:T(8,128)(2,1)}), bf16[112,32,64]{0,2,1:T(8,128)(2,1)S(1)}, u32[]{:S(2)}, u32[]{:S(2)}) %all-to-all-start.5) | async-done | bytes 458784 | tf_op jit(solution)/shard_map/all_to_all | solution.py:105
  211.8 2.3 broadcast_in_dim.14
  214.1 0.0 copy-done.2
  214.1 5.1 %all-to-all-start.1 = ((bf16[8,112,2048]{2,1,0:T(8,128)(2,1)}), bf16[8,112,2048]{2,1,0:T(8,128)(2,1)}, u32[]{:S(2)}, u32[]{:S(2)}) async-start(bf16[8,112,2048]{2,1,0:T(8,128)(2,1)} %broadcast_in_dim.14), calls=%async_computation.1 | async-start | bytes 7340032 | tf_op jit(solution)/shard_map/all_to_all | solution.py:28
  219.2 2.0 fusion.14
  221.3 2.0 fusion.7
  223.3 47.2 %fusion = bf16[16,2048]{1,0:T(8,128)(2,1)S(1)} fusion(bf16[112,2048]{1,0:T(8,128)(2,1)S(1)} %fusion.7), kind=kCustom, calls=%all-reduce-scatter | all-reduce-scatter fusion | flops 262145 | bytes 526336
  270.5 1.9 collective-permute-start
  272.5 0.2 maximum_convert_fusion
  272.7 1.3 dynamic-slice.4
  274.6 0.3 copy.25
  275.0 1.8 all_to_all.48
  276.7 1.4 copy.27
  278.1 1.8 all_to_all.54
  279.9 0.0 collective-permute-done
  279.9 0.2 concatenate.12
  280.1 13.1 %all-gather.1 = bf16[8,14,2048]{2,1,0:T(8,128)(2,1)S(1)} all-gather(bf16[1,14,2048]{2,1,0:T(8,128)(2,1)S(1)} %dynamic-slice_bitcast_fusion), channel_id=2, replica_groups=mesh['rep'=2,'fs'=32,'tp'=8] {'tp'}, dimensions={0}, use_global_device_ids=true | all-gather | bytes 516096 | tf_op jit(solution)/shard_map/all_gather | solution.py:45
  293.2 0.1 reshape.58
  293.4 0.2 multiply_reduce_fusion.1
  293.6 0.0 all-to-all-done.1
  293.6 2.9 convert_reduce_fusion
  296.5 0.0 copy-done.4
  296.5 1.2 add_convert_fusion
  297.7 38.8 %all-gather.4.cloned.1.call-done = bf16[3584,1152]{1,0:T(8,128)(2,1)} async-done(((bf16[112,1152]{1,0:T(8,128)(2,1)}), bf16[3584,1152]{1,0:T(8,128)(2,1)}) %all-gather.4.cloned.1.call-update) | async-done | bytes 8257552 | tf_op jit(solution)/shard_map/all_gather | solution.py:51
  336.5 2.5 fusion.30
  339.0 0.7 broadcast_in_dim.15
  339.7 6.8 %all-to-all-start.3 = ((bf16[2,64,384]{2,1,0:T(8,128)(2,1)}), bf16[2,64,384]{2,1,0:T(8,128)(2,1)S(1)}, u32[]{:S(2)}, u32[]{:S(2)}) async-start(bf16[2,64,384]{2,1,0:T(8,128)(2,1)} %broadcast_in_dim.15), calls=%async_computation.3 | async-start | bytes 196608 | tf_op jit(solution)/shard_map/all_to_all | solution.py:28
  346.5 2.3 fusion.33
  348.8 0.0 copy-start.7
  348.8 0.0 copy-start.8
  348.9 0.0 copy-start.9
  348.9 2.4 fusion.27
  351.2 3.5 all-to-all-done.3
  354.7 0.6 broadcast_in_dim.16
  355.3 3.8 all-to-all-start.4
  359.1 0.7 add.49
  359.8 7.5 %all-to-all-done.4 = bf16[2,64,384]{2,1,0:T(8,128)(2,1)S(1)} async-done(((bf16[2,64,384]{2,1,0:T(8,128)(2,1)}), bf16[2,64,384]{2,1,0:T(8,128)(2,1)S(1)}, u32[]{:S(2)}, u32[]{:S(2)}) %all-to-all-start.4) | async-done | bytes 98336 | tf_op jit(solution)/shard_map/all_to_all | solution.py:28
  367.3 0.6 broadcast_in_dim.17
  368.0 3.3 all-to-all-start.6
  371.3 0.7 add.50
  372.0 7.5 %all-to-all-done.6 = bf16[2,384,64]{1,2,0:T(8,128)(2,1)S(1)} async-done(((bf16[2,384,64]{1,2,0:T(8,128)(2,1)}), bf16[2,384,64]{1,2,0:T(8,128)(2,1)S(1)}, u32[]{:S(2)}, u32[]{:S(2)}) %all-to-all-start.6) | async-done | bytes 98336 | tf_op jit(solution)/shard_map/all_to_all | solution.py:28
  379.5 0.7 add.51
  (21 shorter events, 0.2 us)
Async XLA Ops:
  10.8 13.2 %copy-start = (bf16[112,2048]{1,0:T(8,128)(2,1)S(1)}, bf16[112,2048]{1,0:T(8,128)(2,1)}, u32[]{:S(2)}) copy-start(bf16[112,2048]{1,0:T(8,128)(2,1)} %param.10) | copy-start | bytes 1376260
  10.8 13.2 %copy-start.1 = (bf16[112,2048]{1,0:T(8,128)(2,1)S(1)}, bf16[112,2048]{1,0:T(8,128)(2,1)}, u32[]{:S(2)}) copy-start(bf16[112,2048]{1,0:T(8,128)(2,1)} %param.9) | copy-start | bytes 1376260
  10.8 134.0 %all-to-all-start = ((bf16[32,64,1152]{2,1,0:T(8,128)(2,1)}), bf16[32,64,1152]{2,1,0:T(8,128)(2,1)}, u32[]{:S(2)}, u32[]{:S(2)}) async-start(bf16[32,64,1152]{2,1,0:T(8,128)(2,1)} %stack.2), calls=%async_computation | async-start | bytes 9437184 | tf_op jit(solution)/shard_map/all_to_all | solution.py:14
  24.0 312.5 %all-gather.4.cloned.1.call-start = ((), (), s32[]{:S(2)}) async-start(), calls=%async_computation.7 | async-start | bytes 8515584 | tf_op jit(solution)/shard_map/all_gather | solution.py:51
  146.9 2.2 copy-start.3
  152.8 32.7 %all-to-all-start.2 = ((bf16[112,32,64]{0,2,1:T(8,128)(2,1)}), bf16[112,32,64]{0,2,1:T(8,128)(2,1)S(1)}, u32[]{:S(2)}, u32[]{:S(2)}) async-start(bf16[112,32,64]{0,2,1:T(8,128)(2,1)} %bitcast.4), calls=%async_computation.2 | async-start | bytes 1048576 | tf_op jit(solution)/shard_map/all_to_all | solution.py:104
  185.5 26.4 %all-to-all-start.5 = ((bf16[112,32,64]{0,2,1:T(8,128)(2,1)}), bf16[112,32,64]{0,2,1:T(8,128)(2,1)S(1)}, u32[]{:S(2)}, u32[]{:S(2)}) async-start(bf16[112,32,64]{0,2,1:T(8,128)(2,1)} %bitcast.6), calls=%async_computation.5 | async-start | bytes 1048576 | tf_op jit(solution)/shard_map/all_to_all | solution.py:105
  211.8 2.3 copy-start.2
  214.1 79.5 %all-to-all-start.1 = ((bf16[8,112,2048]{2,1,0:T(8,128)(2,1)}), bf16[8,112,2048]{2,1,0:T(8,128)(2,1)}, u32[]{:S(2)}, u32[]{:S(2)}) async-start(bf16[8,112,2048]{2,1,0:T(8,128)(2,1)} %broadcast_in_dim.14), calls=%async_computation.1 | async-start | bytes 7340032 | tf_op jit(solution)/shard_map/all_to_all | solution.py:28
  270.5 9.4 %collective-permute-start = (bf16[14,2048]{1,0:T(8,128)(2,1)S(1)}, bf16[14,2048]{1,0:T(8,128)(2,1)S(1)}, u32[]{:S(2)}, u32[]{:S(2)}) collective-permute-start(bf16[14,2048]{1,0:T(8,128)(2,1)S(1)} %slice.75), channel_id=1, source_target_pairs={{0,1},{1,2},{2,3},{3,4},{4,5},{5,6},{6,7},{8,9},{9,10},{10,11},{11... | collective-permute-start | bytes 172040
  293.6 2.9 copy-start.4
  297.7 48.8 %copy-start.5 = (bf16[3584,64]{0,1:T(8,128)(2,1)S(1)}, bf16[3584,64]{0,1:T(8,128)(2,1)}, u32[]{:S(2)}) copy-start(bf16[3584,64]{0,1:T(8,128)(2,1)} %all_to_all.48) | copy-start | bytes 1376260
  339.0 9.8 %copy-start.6 = (bf16[3584,64]{0,1:T(8,128)(2,1)S(1)}, bf16[3584,64]{0,1:T(8,128)(2,1)}, u32[]{:S(2)}) copy-start(bf16[3584,64]{0,1:T(8,128)(2,1)} %all_to_all.54) | copy-start | bytes 1376260
  339.7 15.0 %all-to-all-start.3 = ((bf16[2,64,384]{2,1,0:T(8,128)(2,1)}), bf16[2,64,384]{2,1,0:T(8,128)(2,1)S(1)}, u32[]{:S(2)}, u32[]{:S(2)}) async-start(bf16[2,64,384]{2,1,0:T(8,128)(2,1)} %broadcast_in_dim.15), calls=%async_computation.3 | async-start | bytes 196608 | tf_op jit(solution)/shard_map/all_to_all | solution.py:28
  348.8 10.3 %copy-start.7 = (f32[64,384]{1,0:T(8,128)S(1)}, f32[64,384]{1,0:T(8,128)}, u32[]{:S(2)}) copy-start(f32[64,384]{1,0:T(8,128)} %param.15) | copy-start | bytes 294916
  348.8 22.5 %copy-start.8 = (f32[64,384]{1,0:T(8,128)S(1)}, f32[64,384]{1,0:T(8,128)}, u32[]{:S(2)}) copy-start(f32[64,384]{1,0:T(8,128)} %param.16) | copy-start | bytes 294916
  348.9 30.7 %copy-start.9 = (f32[384,64]{0,1:T(8,128)S(1)}, f32[384,64]{0,1:T(8,128)}, u32[]{:S(2)}) copy-start(f32[384,64]{0,1:T(8,128)} %param.17) | copy-start | bytes 294916
  355.3 12.0 %all-to-all-start.4 = ((bf16[2,64,384]{2,1,0:T(8,128)(2,1)}), bf16[2,64,384]{2,1,0:T(8,128)(2,1)S(1)}, u32[]{:S(2)}, u32[]{:S(2)}) async-start(bf16[2,64,384]{2,1,0:T(8,128)(2,1)} %broadcast_in_dim.16), calls=%async_computation.4 | async-start | bytes 196608 | tf_op jit(solution)/shard_map/all_to_all | solution.py:28
  368.0 11.5 %all-to-all-start.6 = ((bf16[2,384,64]{1,2,0:T(8,128)(2,1)}), bf16[2,384,64]{1,2,0:T(8,128)(2,1)S(1)}, u32[]{:S(2)}, u32[]{:S(2)}) async-start(bf16[2,384,64]{1,2,0:T(8,128)(2,1)} %broadcast_in_dim.17), calls=%async_computation.6 | async-start | bytes 196608 | tf_op jit(solution)/shard_map/all_to_all | solution.py:28
Sparse Core Ops, SparseCore 0:
  151.8 184.6 all-gather.3
